TPU v7x, 512 devices: a 8x2x16 block of a 8x8x16 slice. The times are simulated.
512 devices in a mesh: grp: 2 (over y), sp: 16 (over z), dp: 16 (over x, core).
Axes of the slice: x: 8, y: 2, z: 16, core: 2. Of those that a mesh axis runs over, the one named last changes fastest.
The devices are a block of a 8x8x16 slice.
Arguments:
- tokens: bfloat16 [32, 2048, 2048], P(('grp', 'dp'), 'sp'), parts along dimension 0, may hold values from -6 to 6
- forget_offset: float32 [32, 2048], P(('grp', 'dp'), 'sp'), parts along dimension 0, may hold values from -1.2 to 1.2, as said below
- q_weight: bfloat16 [2048, 2048], P(None, 'dp'), may hold values from -0.125 to 0.125
- k_weight: bfloat16 [2048, 512], P(None, 'dp'), may hold values from -0.125 to 0.125
- v_weight: bfloat16 [2048, 512], P(None, 'dp'), may hold values from -0.125 to 0.125
- forget_weight: bfloat16 [2048, 16], replicated, may hold values from -0.125 to 0.125
- forget_bias: float32 [16], replicated, may hold values from 3 to 12
- score_gain: float32 [16], replicated, may hold values from 0.5 to 80
- out_gain: float32 [2048], replicated, may hold values from 0.1 to 1.9
Outputs:
- attended: bfloat16 [32, 2048, 2048], P(('grp', 'dp'), 'sp'), parts along dimension 0
There are 2 independent parts, one for each index of `grp`. A program takes and returns all parts, laid end to end along the dimension named above; an argument that names none is the same for every part. Nothing has to cross between parts.
Inputs may be any that keep to these rules, and one draw needn't show every extreme that they name: `forget_offset`: constant over aligned spans of 64 positions.
All inputs are finite; a program needn't handle non-finite values.
Results may differ from a plain program's by a relative error of at most 0.0085.
The roundings to bfloat16 on the way count: a program that leaves them out, or rounds other values in their place, can miss the bound.
Values may be sent and summed in bfloat16 or wider, within the bound.
No kernel may reach another device: no remote copies, remote signals or barrier semaphores. Data moves between devices by JAX's collectives and lax.ppermute only.
A program may use at most 128 MiB of HBM per device.

v0:
```python
import jax
import jax.numpy as jnp
from jax import lax
from jax.sharding import PartitionSpec as P

NEG = -1e30
QK_FLOOR = 0.1
OUT_FLOOR = 0.001


def turned_gather(arrays, axis, dims):
    turned = [jnp.moveaxis(a, dim, 0) for a, dim in zip(arrays, dims)]
    both = jnp.concatenate([t.reshape(len(t), -1) for t in turned], axis=1)
    whole, at, done = (lax.all_gather(both, axis, axis=0, tiled=True), 0, [])
    for t, dim in zip(turned, dims):
        piece = whole[:, at : at + t[0].size].reshape(-1, *t.shape[1:])
        done.append(jnp.moveaxis(piece, 0, dim))
        at += t[0].size
    return tuple(done)


def head_norm(vectors, floor):
    return vectors * lax.rsqrt(jnp.mean(vectors * vectors, axis=-1, keepdims=True) + floor)


def local(
    tokens,
    forget_offset,
    q_weight,
    k_weight,
    v_weight,
    forget_weight,
    forget_bias,
    score_gain,
    out_gain,
):
    own_rows = tokens[0]
    tok_count = own_rows.shape[0]
    head_count = forget_bias.shape[0]
    head_dim = out_gain.shape[0] // head_count
    kv_heads = k_weight.shape[1] * lax.axis_size("dp") // head_dim
    spread = lax.axis_size("sp")
    local_heads = head_count // spread
    local_kv = max(1, kv_heads // spread)
    group_size = local_heads // local_kv
    queries = jnp.dot(
        own_rows,
        lax.all_gather(q_weight, "dp", axis=1, tiled=True),
        preferred_element_type=jnp.float32,
    ).astype(jnp.bfloat16)
    key_full, value_full = turned_gather((k_weight, v_weight), "dp", (1, 1))
    keys_proj = jnp.dot(own_rows, key_full, preferred_element_type=jnp.float32).astype(jnp.bfloat16)
    values_proj = jnp.dot(own_rows, value_full, preferred_element_type=jnp.float32).astype(
        jnp.bfloat16
    )
    forget_input = (
        jnp.dot(own_rows, forget_weight, preferred_element_type=jnp.float32)
        + forget_offset[0][:, None]
    ).astype(jnp.bfloat16)
    query_send = queries.reshape(tok_count, spread, local_heads, head_dim)
    forget_send = forget_input.reshape(tok_count, spread, local_heads)
    copies = spread // kv_heads
    key_send = jnp.broadcast_to(
        keys_proj.reshape(tok_count, kv_heads, 1, head_dim), (tok_count, kv_heads, copies, head_dim)
    ).reshape(tok_count, spread, 1, head_dim)
    value_send = jnp.broadcast_to(
        values_proj.reshape(tok_count, kv_heads, 1, head_dim),
        (tok_count, kv_heads, copies, head_dim),
    ).reshape(tok_count, spread, 1, head_dim)
    query_head, forget_head, key_head, value_head = (
        lax.all_to_all(query_send, "sp", split_axis=1, concat_axis=0, tiled=True),
        lax.all_to_all(forget_send, "sp", split_axis=1, concat_axis=0, tiled=True),
        lax.all_to_all(key_send, "sp", split_axis=1, concat_axis=0, tiled=True),
        lax.all_to_all(value_send, "sp", split_axis=1, concat_axis=0, tiled=True),
    )
    length = query_head.shape[0]
    first_head = lax.axis_index("sp") * local_heads
    bias_local = lax.dynamic_slice_in_dim(forget_bias, first_head, local_heads, 0)
    gain_local = lax.dynamic_slice_in_dim(score_gain, first_head, local_heads, 0)
    norm_local = lax.dynamic_slice_in_dim(
        out_gain, first_head * head_dim, local_heads * head_dim, 0
    )
    log_gate = jax.nn.log_sigmoid(
        forget_head.reshape(length, local_heads).astype(jnp.float32) + bias_local[None, :]
    )
    cumulative = jnp.cumsum(log_gate, axis=0).reshape(length, local_kv, group_size)
    query_unit = head_norm(query_head.astype(jnp.float32), QK_FLOOR).astype(jnp.bfloat16)
    key_unit = head_norm(
        key_head.reshape(length, local_kv, head_dim).astype(jnp.float32), QK_FLOOR
    ).astype(jnp.bfloat16)
    value_heads = value_head.reshape(length, local_kv, head_dim)
    factor = (gain_local * head_dim ** (-0.5)).reshape(local_kv, group_size)
    out_gains = norm_local.reshape(local_kv, group_size, head_dim)
    key_totals = jnp.transpose(cumulative, (1, 2, 0))
    span_rows = 512
    positions = jnp.arange(length, dtype=jnp.int32)

    def attend_block(block_index):
        first = block_index * span_rows
        query_block = lax.dynamic_slice_in_dim(query_unit, first, span_rows, 0)
        query_totals = lax.dynamic_slice_in_dim(cumulative, first, span_rows, 0)
        scores = jnp.einsum(
            "qkgd,skd->kgqs", query_block, key_unit, preferred_element_type=jnp.float32
        )
        scores = (
            scores * factor[:, :, None, None]
            + jnp.transpose(query_totals, (1, 2, 0))[..., None]
            - key_totals[:, :, None, :]
        )
        allowed = positions[None, :] <= (first + jnp.arange(span_rows, dtype=jnp.int32))[:, None]
        scores = jnp.where(allowed[None, None], scores, NEG)
        row_peak = jnp.max(scores, axis=-1, keepdims=True)
        exponent = jnp.exp(scores - row_peak)
        weights = (exponent / jnp.sum(exponent, axis=-1, keepdims=True)).astype(jnp.bfloat16)
        mixed = jnp.einsum(
            "kgqs,skd->qkgd", weights, value_heads, preferred_element_type=jnp.float32
        )
        return (head_norm(mixed, OUT_FLOOR) * out_gains).astype(jnp.bfloat16)

    outputs = lax.map(attend_block, jnp.arange(length // span_rows, dtype=jnp.int32))
    outputs = outputs.reshape(length, local_heads, head_dim)
    back_rows = lax.all_to_all(outputs, "sp", split_axis=0, concat_axis=1, tiled=True)
    return back_rows.reshape(1, tok_count, head_count * head_dim)


def solution(mesh):
    in_specs = (
        P(("grp", "dp"), "sp", None),
        P(("grp", "dp"), "sp"),
        P(None, "dp"),
        P(None, "dp"),
        P(None, "dp"),
        P(),
        P(),
        P(),
        P(),
    )
    out_specs = P(("grp", "dp"), "sp", None)
    return jax.shard_map(local, mesh=mesh, in_specs=in_specs, out_specs=out_specs, check_vma=False)
```

profile of v0, /device:TPU:66, one launch (start us, length us, event | category | flops | bytes accessed | tf_op | source)
XLA Modules:
  0.0 312.4 jit_solution(6039166641499261542)
XLA Ops:
  6.6 1.7 pad_maximum_fusion
  8.4 0.7 all-gather.3.cloned.1.call-update
  9.2 1.1 fusion.29
  10.3 0.6 copy.52
  10.9 43.7 %all-to-all-start.2 = ((bf16[128,16,1]{0,2,1:T(2,128)(2,1)}), bf16[128,16,1]{0,2,1:T(2,128)(2,1)S(1)}, u32[]{:S(2)}, u32[]{:S(2)}) async-start(bf16[128,16,1]{0,2,1:T(2,128)(2,1)} %copy.52), calls=%async_computation.2 | async-start | bytes 16384 | tf_op jit(solution)/shard_map/all_to_all | solution.py:72
  54.6 36.7 %all-gather.5.cloned.1.call-done = bf16[512,4096]{1,0:T(8,128)(2,1)} async-done(((bf16[32,4096]{1,0:T(8,128)(2,1)}), bf16[512,4096]{1,0:T(8,128)(2,1)}) %all-gather.5.cloned.1.call-update) | async-done | bytes 4194320 | tf_op jit(solution)/shard_map/all_gather | solution.py:14
  91.2 2.3 fusion.22
  93.7 0.9 broadcast_in_dim.36
  94.6 13.1 %all-to-all-start.1 = ((bf16[128,16,1,128]{3,0,2,1:T(8,128)(2,1)}), bf16[128,16,1,128]{3,0,2,1:T(8,128)(2,1)S(1)}, u32[]{:S(2)}, u32[]{:S(2)}) async-start(bf16[128,16,1,128]{3,0,2,1:T(8,128)(2,1)} %bitcast.10), calls=%async_computation.1 | async-start | bytes 1048576 | tf_op jit(solution)/shard_map/all_to_all | solution.py:73
  107.7 56.5 %all-gather.3.cloned.1.call-done = bf16[2048,2048]{1,0:T(8,128)(2,1)} async-done(((bf16[2048,128]{1,0:T(8,128)(2,1)}), bf16[2048,2048]{1,0:T(8,128)(2,1)}) %all-gather.3.cloned.1.call-update) | async-done | bytes 8388624 | tf_op jit(solution)/shard_map/all_gather | solution.py:48
  164.2 4.6 %fusion.21 = bf16[16,8,16,128]{3,1,2,0:T(8,128)(2,1)S(1)} fusion(bf16[2048,2048]{1,0:T(8,128)(2,1)} %all-gather.3.cloned.1.call-done, bf16[1,128,2048]{2,1,0:T(8,128)(2,1)S(1)} %copy-done), kind=kOutput, calls=%fused_computation.29 | convolution fusion | flops 1074003968 | bytes 9437184 | tf_op jit(solution)/shard_map/dot_general | solution.py:46
  169.0 0.9 copy.48
  169.9 11.1 %all-to-all-start = ((bf16[128,16,1,128]{3,0,2,1:T(8,128)(2,1)}), bf16[128,16,1,128]{3,0,2,1:T(8,128)(2,1)S(1)}, u32[]{:S(2)}, u32[]{:S(2)}) async-start(bf16[128,16,1,128]{3,0,2,1:T(8,128)(2,1)} %copy.48), calls=%async_computation | async-start | bytes 1048576 | tf_op jit(solution)/shard_map/all_to_all | solution.py:71
  181.0 0.6 dynamic_slice.19
  181.6 0.6 dynamic_slice.20
  182.2 0.8 dynamic_slice.21
  183.6 0.6 add_negate_fusion
  184.5 2.3 fusion.25
  186.9 23.1 %all-to-all-done = bf16[128,16,1,128]{3,0,2,1:T(8,128)(2,1)S(1)} async-done(((bf16[128,16,1,128]{3,0,2,1:T(8,128)(2,1)}), bf16[128,16,1,128]{3,0,2,1:T(8,128)(2,1)S(1)}, u32[]{:S(2)}, u32[]{:S(2)}) %all-to-all-start) | async-done | bytes 524320 | tf_op jit(solution)/shard_map/all_to_all | solution.py:71
  210.0 0.9 broadcast_in_dim.38
  210.9 6.8 %all-to-all-start.3 = ((bf16[128,16,1,128]{3,0,2,1:T(8,128)(2,1)}), bf16[128,16,1,128]{3,0,2,1:T(8,128)(2,1)S(1)}, u32[]{:S(2)}, u32[]{:S(2)}) async-start(bf16[128,16,1,128]{3,0,2,1:T(8,128)(2,1)} %bitcast.31), calls=%async_computation.3 | async-start | bytes 1048576 | tf_op jit(solution)/shard_map/all_to_all | solution.py:74
  218.3 0.3 multiply_reduce_fusion.1
  218.7 0.3 multiply_convert_fusion.1
  219.1 0.3 multiply_reduce_fusion.2
  219.5 0.3 multiply_convert_fusion.2
  219.8 26.8 %all-to-all-done.3 = bf16[128,16,1,128]{3,0,2,1:T(8,128)(2,1)S(1)} async-done(((bf16[128,16,1,128]{3,0,2,1:T(8,128)(2,1)}), bf16[128,16,1,128]{3,0,2,1:T(8,128)(2,1)S(1)}, u32[]{:S(2)}, u32[]{:S(2)}) %all-to-all-start.3) | async-done | bytes 524320 | tf_op jit(solution)/shard_map/all_to_all | solution.py:74
  246.6 19.9 %while.11 = (s32[]{:T(128)}, bf16[4,512,1,1,128]{4,1,0,3,2:T(8,128)(2,1)S(1)}, s32[4]{0:T(128)S(1)}, bf16[2048,1,1,128]{3,0,2,1:T(8,128)(2,1)S(1)}, bf16[2048,1,...) while((s32[]{:T(128)}, ...), condition=%wide.region_8.9_spmd.clone, body=%wide.region_4.8_spmd.clone.sunk | while | flops 548732928 | bytes 14979803 | solution.py:120
  246.6 0.6 dynamic_slice.37
  247.9 1.3 fusion.41
  249.2 0.7 fusion.42
  249.9 1.4 multiply_reduce_fusion.4
  251.6 0.6 dynamic_slice.37
  252.9 1.3 fusion.41
  254.2 0.7 fusion.42
  254.9 1.4 multiply_reduce_fusion.4
  256.6 0.6 dynamic_slice.37
  257.9 1.3 fusion.41
  259.1 0.7 fusion.42
  259.9 1.4 multiply_reduce_fusion.4
  261.6 0.6 dynamic_slice.37
  262.9 1.3 fusion.41
  264.1 0.7 fusion.42
  264.8 1.4 multiply_reduce_fusion.4
  266.6 0.5 broadcast.193
  267.1 1.0 reduce.14
  268.2 35.4 %all_to_all.57 = bf16[16,2,8192]{2,1,0:T(2,128)(2,1)S(1)} all-to-all(bf16[16,2,8192]{2,1,0:T(2,128)(2,1)S(1)} %reshape.438), channel_id=1, replica_groups=mesh['grp'=2,'sp'=16,'dp'=16] {'sp'}, dimensions={0} | all-to-all | bytes 1048576 | tf_op jit(solution)/shard_map/all_to_all | solution.py:122
  303.6 0.5 reshape.439
  304.5 1.0 copy.57
  (55 shorter events, 3.0 us)
Async XLA Ops:
  6.5 2.6 copy-start
  6.6 84.7 %all-gather.5.cloned.1.call-start = ((), (), s32[]{:S(2)}) async-start(), calls=%async_computation.6 | async-start | bytes 4456448 | tf_op jit(solution)/shard_map/all_gather | solution.py:14
  8.4 155.8 %all-gather.3.cloned.1.call-start = ((), (), s32[]{:S(2)}) async-start(), calls=%async_computation.5 | async-start | bytes 8912896 | tf_op jit(solution)/shard_map/all_gather | solution.py:48
  10.9 82.8 %all-to-all-start.2 = ((bf16[128,16,1]{0,2,1:T(2,128)(2,1)}), bf16[128,16,1]{0,2,1:T(2,128)(2,1)S(1)}, u32[]{:S(2)}, u32[]{:S(2)}) async-start(bf16[128,16,1]{0,2,1:T(2,128)(2,1)} %copy.52), calls=%async_computation.2 | async-start | bytes 16384 | tf_op jit(solution)/shard_map/all_to_all | solution.py:72
  94.6 75.3 %all-to-all-start.1 = ((bf16[128,16,1,128]{3,0,2,1:T(8,128)(2,1)}), bf16[128,16,1,128]{3,0,2,1:T(8,128)(2,1)S(1)}, u32[]{:S(2)}, u32[]{:S(2)}) async-start(bf16[128,16,1,128]{3,0,2,1:T(8,128)(2,1)} %bitcast.10), calls=%async_computation.1 | async-start | bytes 1048576 | tf_op jit(solution)/shard_map/all_to_all | solution.py:73
  107.7 73.3 %copy-start.1 = (f32[16]{0:T(128)S(1)}, f32[16]{0:T(128)}, u32[]{:S(2)}) copy-start(f32[16]{0:T(128)} %param.18) | copy-start | bytes 196
  107.7 73.9 %copy-start.2 = (f32[16]{0:T(128)S(1)}, f32[16]{0:T(128)}, u32[]{:S(2)}) copy-start(f32[16]{0:T(128)} %param.17) | copy-start | bytes 196
  169.9 40.1 %all-to-all-start = ((bf16[128,16,1,128]{3,0,2,1:T(8,128)(2,1)}), bf16[128,16,1,128]{3,0,2,1:T(8,128)(2,1)S(1)}, u32[]{:S(2)}, u32[]{:S(2)}) async-start(bf16[128,16,1,128]{3,0,2,1:T(8,128)(2,1)} %copy.48), calls=%async_computation | async-start | bytes 1048576 | tf_op jit(solution)/shard_map/all_to_all | solution.py:71
  210.9 35.7 %all-to-all-start.3 = ((bf16[128,16,1,128]{3,0,2,1:T(8,128)(2,1)}), bf16[128,16,1,128]{3,0,2,1:T(8,128)(2,1)S(1)}, u32[]{:S(2)}, u32[]{:S(2)}) async-start(bf16[128,16,1,128]{3,0,2,1:T(8,128)(2,1)} %bitcast.31), calls=%async_computation.3 | async-start | bytes 1048576 | tf_op jit(solution)/shard_map/all_to_all | solution.py:74
Sparse Core Ops, SparseCore 0:
  9.5 81.7 all-gather.4
  93.3 70.8 all-gather.2
where the time goes:
time: 313 us; the launch traced here: 312 us
  waiting for transfers between devices  144 us (46%)
  starting transfers between devices  74.7 us (24%)
  blocking collectives  35.4 us (11%)
  matrix products  21.2 us (7%)
  between operations  14.3 us (5%)
  local copies, waits for them, and re-layouts  11.5 us (4%)
  other arithmetic  8.64 us (3%)
    all_gather x1, waiting for transfers between devices, local(): lax.all_gather(q_weight, 'dp', axis=1, tiled=True)  56.5 us
    all_to_all x1, starting transfers between devices, local(): lax.all_to_all(forget_send, 'sp', split_axis=1, concat_axis=0, tiled=True)  43.7 us
    all_gather x1, waiting for transfers between devices, turned_gather(): whole, at, done = (lax.all_gather(both, axis, axis=0, tiled=True), 0, [])  36.7 us
    all_to_all x1, blocking collectives, local(): lax.all_to_all(outputs, 'sp', split_axis=0, concat_axis=1, tiled=True)  35.4 us
    all_to_all x1, waiting for transfers between devices, local(): lax.all_to_all(value_send, 'sp', split_axis=1, concat_axis=0, tiled=True)  26.8 us
    all_to_all x1, waiting for transfers between devices, local(): lax.all_to_all(query_send, 'sp', split_axis=1, concat_axis=0, tiled=True)  23.1 us
    all_to_all x1, starting transfers between devices, local(): lax.all_to_all(key_send, 'sp', split_axis=1, concat_axis=0, tiled=True)  13.1 us
    all_to_all x1, starting transfers between devices, local(): lax.all_to_all(query_send, 'sp', split_axis=1, concat_axis=0, tiled=True)  11.1 us
  transfers between devices with their start and end apart: 6, of which 4 were waited for; matrix products, arithmetic and copies ran while one was open for 6% of the time, Pallas kernels for 0%

commit v1 on v0

--- a/solution.py
+++ b/solution.py
@@ -6,6 +6,28 @@
 NEG = -1e30
 QK_FLOOR = 0.1
 OUT_FLOOR = 0.001
+
+
+def joined_along(blocks, dim):
+    dims = list(blocks.shape[1:])
+    dims[dim] *= blocks.shape[0]
+    return jnp.moveaxis(blocks, 0, dim).reshape(dims)
+
+
+def gather_around(array, axis, dim):
+    size = lax.axis_size(axis)
+    pairs = [(i, (i + 1) % size) for i in range(size)]
+    back = [(b, a) for a, b in pairs]
+    lower, upper = ([], [])
+    for step in range(size - 1):
+        if step % 2 == 0:
+            lower.append(lax.ppermute(lower[-1] if lower else array, axis, pairs))
+        else:
+            upper.append(lax.ppermute(upper[-1] if upper else array, axis, back))
+    pieces = jnp.stack([*lower[::-1], array, *upper])
+    shift = lax.axis_index(axis) - len(lower)
+    pieces = pieces[(jnp.arange(size) - shift) % size]
+    return joined_along(pieces, dim)
 
 
 def turned_gather(arrays, axis, dims):
@@ -44,9 +66,7 @@
     local_kv = max(1, kv_heads // spread)
     group_size = local_heads // local_kv
     queries = jnp.dot(
-        own_rows,
-        lax.all_gather(q_weight, "dp", axis=1, tiled=True),
-        preferred_element_type=jnp.float32,
+        own_rows, gather_around(q_weight, "dp", 1), preferred_element_type=jnp.float32
     ).astype(jnp.bfloat16)
     key_full, value_full = turned_gather((k_weight, v_weight), "dp", (1, 1))
     keys_proj = jnp.dot(own_rows, key_full, preferred_element_type=jnp.float32).astype(jnp.bfloat16)

time: 313 us -> 356 us (1.14)
  the two profiles are of different devices: /device:TPU:66 before, /device:TPU:86 now
where the time goes in v1:
time: 356 us; the launch traced here: 354 us
  waiting for transfers between devices  107 us (30%)
  starting transfers between devices  104 us (29%)
  local copies, waits for them, and re-layouts  57.9 us (16%)
  blocking collectives  35.4 us (10%)
  matrix products  23.1 us (6%)
  between operations  14.4 us (4%)
  other arithmetic  9.6 us (3%)
    all_to_all x1, starting transfers between devices, local(): lax.all_to_all(forget_send, 'sp', split_axis=1, concat_axis=0, tiled=True)  43.7 us
    all_to_all x1, blocking collectives, local(): lax.all_to_all(outputs, 'sp', split_axis=0, concat_axis=1, tiled=True)  35.4 us
    ppermute x8, waiting for transfers between devices, gather_around(): lower.append(lax.ppermute(lower[-1] if lower else array, axis, pairs))  35.2 us
    all_to_all x1, waiting for transfers between devices, local(): lax.all_to_all(value_send, 'sp', split_axis=1, concat_axis=0, tiled=True)  26.7 us
    ppermute x8, starting transfers between devices, gather_around(): lower.append(lax.ppermute(lower[-1] if lower else array, axis, pairs))  24.6 us
    all_to_all x1, waiting for transfers between devices, local(): lax.all_to_all(key_send, 'sp', split_axis=1, concat_axis=0, tiled=True)  23.4 us
    unnamed x36, local copies, waits for them, and re-layouts  23.4 us
    all_to_all x1, waiting for transfers between devices, local(): lax.all_to_all(query_send, 'sp', split_axis=1, concat_axis=0, tiled=True)  20.5 us
  transfers between devices with their start and end apart: 20, of which 11 were waited for; matrix products, arithmetic and copies ran while one was open for 18% of the time, Pallas kernels for 0%

profile of v1, /device:TPU:86, one launch (start us, length us, event | category | flops | bytes accessed | tf_op | source)
XLA Modules:
  0.0 354.1 jit_solution(16044894735676828040)
XLA Ops:
  6.6 8.8 %collective-permute-done = bf16[2048,128]{1,0:T(8,128)(2,1)S(1)} collective-permute-done((bf16[2048,128]{1,0:T(8,128)(2,1)}, bf16[2048,128]{1,0:T(8,128)(2,1)S(1)}, u32[]{:S(2)}, u32[]{:S(2)}) %collective-permute-start) | collective-permute-done | bytes 524320 | tf_op jit(solution)/shard_map/ppermute | solution.py:24
  15.9 1.2 collective-permute-start.8
  17.1 6.9 %collective-permute-done.1 = bf16[2048,128]{1,0:T(8,128)(2,1)S(1)} collective-permute-done((bf16[2048,128]{1,0:T(8,128)(2,1)S(1)}, bf16[2048,128]{1,0:T(8,128)(2,1)S(1)}, u32[]{:S(2)}, u32[]{:S(2)}) %collective-permute-start.1) | collective-permute-done | bytes 524320 | tf_op jit(solution)/shard_map/ppermute | solution.py:24
  24.0 1.7 collective-permute-start.2
  25.9 6.6 %collective-permute-done.2 = bf16[2048,128]{1,0:T(8,128)(2,1)S(1)} collective-permute-done((bf16[2048,128]{1,0:T(8,128)(2,1)S(1)}, bf16[2048,128]{1,0:T(8,128)(2,1)S(1)}, u32[]{:S(2)}, u32[]{:S(2)}) %collective-permute-start.2) | collective-permute-done | bytes 524320 | tf_op jit(solution)/shard_map/ppermute | solution.py:24
  32.6 2.9 collective-permute-start.3
  35.5 5.7 %collective-permute-done.3 = bf16[2048,128]{1,0:T(8,128)(2,1)S(1)} collective-permute-done((bf16[2048,128]{1,0:T(8,128)(2,1)S(1)}, bf16[2048,128]{1,0:T(8,128)(2,1)S(1)}, u32[]{:S(2)}, u32[]{:S(2)}) %collective-permute-start.3) | collective-permute-done | bytes 524320 | tf_op jit(solution)/shard_map/ppermute | solution.py:24
  41.2 4.1 %collective-permute-start.4 = (bf16[2048,128]{1,0:T(8,128)(2,1)S(1)}, bf16[2048,128]{1,0:T(8,128)(2,1)S(1)}, u32[]{:S(2)}, u32[]{:S(2)}) collective-permute-start(bf16[2048,128]{1,0:T(8,128)(2,1)S(1)} %collective-permute-done.3), channel_id=1, source_target_pairs={{0,1},{1,2},{2,3},{3,4},{4,5},{5,6},{6,7},{7,8},{8,9},{9,10},{10,1... | collective-permute-start | bytes 1572872 | tf_op jit(solution)/shard_map/ppermute | solution.py:24
  46.1 3.7 %collective-permute-done.4 = bf16[2048,128]{1,0:T(8,128)(2,1)S(1)} collective-permute-done((bf16[2048,128]{1,0:T(8,128)(2,1)S(1)}, bf16[2048,128]{1,0:T(8,128)(2,1)S(1)}, u32[]{:S(2)}, u32[]{:S(2)}) %collective-permute-start.4) | collective-permute-done | bytes 524320 | tf_op jit(solution)/shard_map/ppermute | solution.py:24
  49.8 5.3 %collective-permute-start.5 = (bf16[2048,128]{1,0:T(8,128)(2,1)S(1)}, bf16[2048,128]{1,0:T(8,128)(2,1)}, u32[]{:S(2)}, u32[]{:S(2)}) collective-permute-start(bf16[2048,128]{1,0:T(8,128)(2,1)S(1)} %collective-permute-done.4), channel_id=1, source_target_pairs={{0,1},{1,2},{2,3},{3,4},{4,5},{5,6},{6,7},{7,8},{8,9},{9,10},{10,1... | collective-permute-start | bytes 1572872 | tf_op jit(solution)/shard_map/ppermute | solution.py:24
  55.1 3.4 collective-permute-done.5
  58.5 6.4 %collective-permute-start.6 = (bf16[2048,128]{1,0:T(8,128)(2,1)}, bf16[2048,128]{1,0:T(8,128)(2,1)}, u32[]{:S(2)}, u32[]{:S(2)}) collective-permute-start(bf16[2048,128]{1,0:T(8,128)(2,1)} %collective-permute-done.5), channel_id=1, source_target_pairs={{0,1},{1,2},{2,3},{3,4},{4,5},{5,6},{6,7},{7,8},{8,9},{9,10},{10,1... | collective-permute-start | bytes 1572872 | tf_op jit(solution)/shard_map/ppermute | solution.py:24
  66.6 43.7 %all-to-all-start.2 = ((bf16[128,16,1]{0,2,1:T(2,128)(2,1)}), bf16[128,16,1]{0,2,1:T(2,128)(2,1)S(1)}, u32[]{:S(2)}, u32[]{:S(2)}) async-start(bf16[128,16,1]{0,2,1:T(2,128)(2,1)} %copy.37), calls=%async_computation.2 | async-start | bytes 16384 | tf_op jit(solution)/shard_map/all_to_all | solution.py:92
  110.5 3.6 %collective-permute-start.7 = (bf16[2048,128]{1,0:T(8,128)(2,1)}, bf16[2048,128]{1,0:T(8,128)(2,1)}, u32[]{:S(2)}, u32[]{:S(2)}) collective-permute-start(bf16[2048,128]{1,0:T(8,128)(2,1)} %collective-permute-done.6), channel_id=1, source_target_pairs={{0,1},{1,2},{2,3},{3,4},{4,5},{5,6},{6,7},{7,8},{8,9},{9,10},{10,1... | collective-permute-start | bytes 1572872 | tf_op jit(solution)/shard_map/ppermute | solution.py:24
  114.1 1.7 pad_maximum_fusion
  115.9 1.6 collective-permute-done.13
  117.5 1.9 collective-permute-start.14
  119.5 1.9 bitcast_dynamic-update-slice_fusion.15
  121.3 1.9 bitcast_dynamic-update-slice_fusion.14
  123.2 1.9 bitcast_dynamic-update-slice_fusion.13
  125.1 1.9 bitcast_dynamic-update-slice_fusion.12
  126.9 1.9 bitcast_dynamic-update-slice_fusion.11
  128.8 1.9 bitcast_dynamic-update-slice_fusion.10
  135.7 1.9 bitcast_dynamic-update-slice_fusion.3
  137.6 1.9 bitcast_dynamic-update-slice_fusion.2
  139.5 1.9 bitcast_dynamic-update-slice_fusion.1
  142.3 8.4 %gather_fusion = bf16[16,2048,128]{2,1,0:T(8,128)(2,1)} fusion(bf16[16,2048,128]{2,1,0:T(8,128)(2,1)} %bitcast_dynamic-update-slice_fusion, s32[1024]{0:T(1024)S(1)} %pad_clamp_fusion), kind=kCustom, calls=%fused_computation | custom fusion | bytes 16777280 | tf_op jit(solution)/shard_map/gather | solution.py:29
  150.6 12.4 %copy.33 = bf16[2048,16,128]{0,2,1:T(8,128)(2,1)} copy(bf16[2048,16,128]{2,0,1:T(8,128)(2,1)} %bitcast.175) | data formatting | bytes 16777216 | tf_op jit(solution)/shard_map/transpose | solution.py:14
  163.0 6.6 %convolution_convert_fusion = bf16[2048,128]{1,0:T(8,128)(2,1)} fusion(bf16[2048,2048]{0,1:T(8,128)(2,1)} %bitcast.176, bf16[1,128,2048]{2,1,0:T(8,128)(2,1)S(1)} %copy-done), kind=kOutput, calls=%fused_computation.25 | convolution fusion | flops 1074003968 | bytes 9437184 | tf_op jit(solution)/shard_map/dot_general | solution.py:68
  169.6 12.0 %all-to-all-start = ((bf16[128,16,1,128]{0,3,2,1:T(8,128)(2,1)}), bf16[128,16,1,128]{0,3,2,1:T(8,128)(2,1)S(1)}, u32[]{:S(2)}, u32[]{:S(2)}) async-start(bf16[128,16,1,128]{0,3,2,1:T(8,128)(2,1)} %bitcast.22), calls=%async_computation | async-start | bytes 1048576 | tf_op jit(solution)/shard_map/all_to_all | solution.py:91
  181.7 2.3 fusion.21
  184.1 20.5 %all-to-all-done = bf16[128,16,1,128]{0,3,2,1:T(8,128)(2,1)S(1)} async-done(((bf16[128,16,1,128]{0,3,2,1:T(8,128)(2,1)}), bf16[128,16,1,128]{0,3,2,1:T(8,128)(2,1)S(1)}, u32[]{:S(2)}, u32[]{:S(2)}) %all-to-all-start) | async-done | bytes 524320 | tf_op jit(solution)/shard_map/all_to_all | solution.py:91
  205.5 12.9 %all-to-all-start.1 = ((bf16[128,16,1,128]{3,0,2,1:T(8,128)(2,1)}), bf16[128,16,1,128]{3,0,2,1:T(8,128)(2,1)S(1)}, u32[]{:S(2)}, u32[]{:S(2)}) async-start(bf16[128,16,1,128]{3,0,2,1:T(8,128)(2,1)} %bitcast.32), calls=%async_computation.1 | async-start | bytes 1048576 | tf_op jit(solution)/shard_map/all_to_all | solution.py:93
  222.0 2.3 fusion.24
  224.5 23.4 %all-to-all-done.1 = bf16[128,16,1,128]{3,0,2,1:T(8,128)(2,1)S(1)} async-done(((bf16[128,16,1,128]{3,0,2,1:T(8,128)(2,1)}), bf16[128,16,1,128]{3,0,2,1:T(8,128)(2,1)S(1)}, u32[]{:S(2)}, u32[]{:S(2)}) %all-to-all-start.1) | async-done | bytes 524320 | tf_op jit(solution)/shard_map/all_to_all | solution.py:93
  248.8 6.9 %all-to-all-start.3 = ((bf16[128,16,1,128]{3,0,2,1:T(8,128)(2,1)}), bf16[128,16,1,128]{3,0,2,1:T(8,128)(2,1)S(1)}, u32[]{:S(2)}, u32[]{:S(2)}) async-start(bf16[128,16,1,128]{3,0,2,1:T(8,128)(2,1)} %bitcast.53), calls=%async_computation.3 | async-start | bytes 1048576 | tf_op jit(solution)/shard_map/all_to_all | solution.py:94
  258.0 26.7 %all-to-all-done.3 = bf16[128,16,1,128]{3,0,2,1:T(8,128)(2,1)S(1)} async-done(((bf16[128,16,1,128]{3,0,2,1:T(8,128)(2,1)}), bf16[128,16,1,128]{3,0,2,1:T(8,128)(2,1)S(1)}, u32[]{:S(2)}, u32[]{:S(2)}) %all-to-all-start.3) | async-done | bytes 524320 | tf_op jit(solution)/shard_map/all_to_all | solution.py:94
  284.6 22.6 %while.11 = (s32[]{:T(128)}, bf16[4,512,1,1,128]{4,1,0,3,2:T(8,128)(2,1)}, s32[4]{0:T(128)S(1)}, bf16[2048,1,1,128]{3,0,2,1:T(8,128)(2,1)S(1)}, bf16[2048,1,128]...) while((s32[]{:T(128)}, ...), condition=%wide.region_8.9_spmd.clone, body=%wide.region_4.8_spmd.clone.sunk | while | flops 548732928 | bytes 14980303 | solution.py:140
  285.9 1.3 fusion.43
  287.9 1.5 multiply_reduce_fusion.4
  291.6 1.2 fusion.43
  293.5 1.5 multiply_reduce_fusion.4
  297.2 1.3 fusion.43
  299.2 1.5 multiply_reduce_fusion.4
  302.8 1.2 fusion.43
  304.8 1.5 multiply_reduce_fusion.4
  307.8 2.0 reduce.14
  309.9 35.4 %all_to_all.57 = bf16[16,2,8192]{2,1,0:T(2,128)(2,1)S(1)} all-to-all(bf16[16,2,8192]{2,1,0:T(2,128)(2,1)S(1)} %reshape.499), channel_id=1, replica_groups=mesh['grp'=2,'sp'=16,'dp'=16] {'sp'}, dimensions={0} | all-to-all | bytes 1048576 | tf_op jit(solution)/shard_map/all_to_all | solution.py:142
  (112 shorter events, 28.4 us)
Async XLA Ops:
  6.5 58.4 %copy-start = (bf16[1,128,2048]{2,1,0:T(8,128)(2,1)S(1)}, bf16[1,128,2048]{2,1,0:T(8,128)(2,1)}, u32[]{:S(2)}) copy-start(bf16[1,128,2048]{2,1,0:T(8,128)(2,1)} %param.11) | copy-start | bytes 1572868
  6.6 125.8 %copy-start.1 = (bf16[2048,128]{1,0:T(8,128)(2,1)S(1)}, bf16[2048,128]{1,0:T(8,128)(2,1)}, u32[]{:S(2)}) copy-start(bf16[2048,128]{1,0:T(8,128)(2,1)} %param.13) | copy-start | bytes 1572868
  6.6 8.8 %collective-permute-start = (bf16[2048,128]{1,0:T(8,128)(2,1)}, bf16[2048,128]{1,0:T(8,128)(2,1)S(1)}, u32[]{:S(2)}, u32[]{:S(2)}) collective-permute-start(bf16[2048,128]{1,0:T(8,128)(2,1)} %param.13), channel_id=1, source_target_pairs={{0,1},{1,2},{2,3},{3,4},{4,5},{5,6},{6,7},{7,8},{8,9},{9,10},{10,1... | collective-permute-start | bytes 1572872 | tf_op jit(solution)/shard_map/ppermute | solution.py:24
  15.4 8.6 %collective-permute-start.1 = (bf16[2048,128]{1,0:T(8,128)(2,1)S(1)}, bf16[2048,128]{1,0:T(8,128)(2,1)S(1)}, u32[]{:S(2)}, u32[]{:S(2)}) collective-permute-start(bf16[2048,128]{1,0:T(8,128)(2,1)S(1)} %collective-permute-done), channel_id=1, source_target_pairs={{0,1},{1,2},{2,3},{3,4},{4,5},{5,6},{6,7},{7,8},{8,9},{9,10},{10,1... | collective-permute-start | bytes 1572872 | tf_op jit(solution)/shard_map/ppermute | solution.py:24
  15.9 9.7 %collective-permute-start.8 = (bf16[2048,128]{1,0:T(8,128)(2,1)}, bf16[2048,128]{1,0:T(8,128)(2,1)S(1)}, u32[]{:S(2)}, u32[]{:S(2)}) collective-permute-start(bf16[2048,128]{1,0:T(8,128)(2,1)} %param.13), channel_id=1, source_target_pairs={{1,0},{2,1},{3,2},{4,3},{5,4},{6,5},{7,6},{8,7},{9,8},{10,9},{11,1... | collective-permute-start | bytes 1572872 | tf_op jit(solution)/shard_map/ppermute | solution.py:26
  24.0 8.6 %collective-permute-start.2 = (bf16[2048,128]{1,0:T(8,128)(2,1)S(1)}, bf16[2048,128]{1,0:T(8,128)(2,1)S(1)}, u32[]{:S(2)}, u32[]{:S(2)}) collective-permute-start(bf16[2048,128]{1,0:T(8,128)(2,1)S(1)} %collective-permute-done.1), channel_id=1, source_target_pairs={{0,1},{1,2},{2,3},{3,4},{4,5},{5,6},{6,7},{7,8},{8,9},{9,10},{10,1... | collective-permute-start | bytes 1572872 | tf_op jit(solution)/shard_map/ppermute | solution.py:24
  25.7 9.8 %collective-permute-start.9 = (bf16[2048,128]{1,0:T(8,128)(2,1)S(1)}, bf16[2048,128]{1,0:T(8,128)(2,1)S(1)}, u32[]{:S(2)}, u32[]{:S(2)}) collective-permute-start(bf16[2048,128]{1,0:T(8,128)(2,1)S(1)} %collective-permute-done.8), channel_id=1, source_target_pairs={{1,0},{2,1},{3,2},{4,3},{5,4},{6,5},{7,6},{8,7},{9,8},{10,9},{11,1... | collective-permute-start | bytes 1572872 | tf_op jit(solution)/shard_map/ppermute | solution.py:26
  32.6 12.7 %copy-start.2 = (bf16[2048,128]{1,0:T(8,128)(2,1)}, bf16[2048,128]{1,0:T(8,128)(2,1)S(1)}, u32[]{:S(2)}) copy-start(bf16[2048,128]{1,0:T(8,128)(2,1)S(1)} %collective-permute-done.2) | copy-start | bytes 1572868
  32.6 8.6 %collective-permute-start.3 = (bf16[2048,128]{1,0:T(8,128)(2,1)S(1)}, bf16[2048,128]{1,0:T(8,128)(2,1)S(1)}, u32[]{:S(2)}, u32[]{:S(2)}) collective-permute-start(bf16[2048,128]{1,0:T(8,128)(2,1)S(1)} %collective-permute-done.2), channel_id=1, source_target_pairs={{0,1},{1,2},{2,3},{3,4},{4,5},{5,6},{6,7},{7,8},{8,9},{9,10},{10,1... | collective-permute-start | bytes 1572872 | tf_op jit(solution)/shard_map/ppermute | solution.py:24
  35.5 9.8 %collective-permute-start.10 = (bf16[2048,128]{1,0:T(8,128)(2,1)S(1)}, bf16[2048,128]{1,0:T(8,128)(2,1)S(1)}, u32[]{:S(2)}, u32[]{:S(2)}) collective-permute-start(bf16[2048,128]{1,0:T(8,128)(2,1)S(1)} %collective-permute-done.9), channel_id=1, source_target_pairs={{1,0},{2,1},{3,2},{4,3},{5,4},{6,5},{7,6},{8,7},{9,8},{10,9},{11,1... | collective-permute-start | bytes 1572872 | tf_op jit(solution)/shard_map/ppermute | solution.py:26
  41.2 13.9 %copy-start.5 = (bf16[2048,128]{1,0:T(8,128)(2,1)}, bf16[2048,128]{1,0:T(8,128)(2,1)S(1)}, u32[]{:S(2)}) copy-start(bf16[2048,128]{1,0:T(8,128)(2,1)S(1)} %collective-permute-done.3) | copy-start | bytes 1572868
  41.2 8.6 %collective-permute-start.4 = (bf16[2048,128]{1,0:T(8,128)(2,1)S(1)}, bf16[2048,128]{1,0:T(8,128)(2,1)S(1)}, u32[]{:S(2)}, u32[]{:S(2)}) collective-permute-start(bf16[2048,128]{1,0:T(8,128)(2,1)S(1)} %collective-permute-done.3), channel_id=1, source_target_pairs={{0,1},{1,2},{2,3},{3,4},{4,5},{5,6},{6,7},{7,8},{8,9},{9,10},{10,1... | collective-permute-start | bytes 1572872 | tf_op jit(solution)/shard_map/ppermute | solution.py:24
  45.3 0.8 copy-start.3
  45.3 9.8 %collective-permute-start.11 = (bf16[2048,128]{1,0:T(8,128)(2,1)S(1)}, bf16[2048,128]{1,0:T(8,128)(2,1)}, u32[]{:S(2)}, u32[]{:S(2)}) collective-permute-start(bf16[2048,128]{1,0:T(8,128)(2,1)S(1)} %collective-permute-done.10), channel_id=1, source_target_pairs={{1,0},{2,1},{3,2},{4,3},{5,4},{6,5},{7,6},{8,7},{9,8},{10,9},{11,1... | collective-permute-start | bytes 1572872 | tf_op jit(solution)/shard_map/ppermute | solution.py:26
  49.8 5.3 %copy-start.6 = (bf16[2048,128]{1,0:T(8,128)(2,1)}, bf16[2048,128]{1,0:T(8,128)(2,1)S(1)}, u32[]{:S(2)}) copy-start(bf16[2048,128]{1,0:T(8,128)(2,1)S(1)} %collective-permute-done.4) | copy-start | bytes 1572868
  49.8 8.7 %collective-permute-start.5 = (bf16[2048,128]{1,0:T(8,128)(2,1)S(1)}, bf16[2048,128]{1,0:T(8,128)(2,1)}, u32[]{:S(2)}, u32[]{:S(2)}) collective-permute-start(bf16[2048,128]{1,0:T(8,128)(2,1)S(1)} %collective-permute-done.4), channel_id=1, source_target_pairs={{0,1},{1,2},{2,3},{3,4},{4,5},{5,6},{6,7},{7,8},{8,9},{9,10},{10,1... | collective-permute-start | bytes 1572872 | tf_op jit(solution)/shard_map/ppermute | solution.py:24
  55.1 55.3 %collective-permute-start.12 = (bf16[2048,128]{1,0:T(8,128)(2,1)}, bf16[2048,128]{1,0:T(8,128)(2,1)}, u32[]{:S(2)}, u32[]{:S(2)}) collective-permute-start(bf16[2048,128]{1,0:T(8,128)(2,1)} %collective-permute-done.11), channel_id=1, source_target_pairs={{1,0},{2,1},{3,2},{4,3},{5,4},{6,5},{7,6},{8,7},{9,8},{10,9},{11,1... | collective-permute-start | bytes 1572872 | tf_op jit(solution)/shard_map/ppermute | solution.py:26
  58.5 52.0 %collective-permute-start.6 = (bf16[2048,128]{1,0:T(8,128)(2,1)}, bf16[2048,128]{1,0:T(8,128)(2,1)}, u32[]{:S(2)}, u32[]{:S(2)}) collective-permute-start(bf16[2048,128]{1,0:T(8,128)(2,1)} %collective-permute-done.5), channel_id=1, source_target_pairs={{0,1},{1,2},{2,3},{3,4},{4,5},{5,6},{6,7},{7,8},{8,9},{9,10},{10,1... | collective-permute-start | bytes 1572872 | tf_op jit(solution)/shard_map/ppermute | solution.py:24
  66.6 103.0 %all-to-all-start.2 = ((bf16[128,16,1]{0,2,1:T(2,128)(2,1)}), bf16[128,16,1]{0,2,1:T(2,128)(2,1)S(1)}, u32[]{:S(2)}, u32[]{:S(2)}) async-start(bf16[128,16,1]{0,2,1:T(2,128)(2,1)} %copy.37), calls=%async_computation.2 | async-start | bytes 16384 | tf_op jit(solution)/shard_map/all_to_all | solution.py:92
  110.3 71.3 %all-gather.2.cloned.1.call-start = ((), (), s32[]{:S(2)}) async-start(), calls=%async_computation.5 | async-start | bytes 4456448 | tf_op jit(solution)/shard_map/all_gather | solution.py:36
  110.4 7.1 %collective-permute-start.13 = (bf16[2048,128]{1,0:T(8,128)(2,1)}, bf16[2048,128]{1,0:T(8,128)(2,1)}, u32[]{:S(2)}, u32[]{:S(2)}) collective-permute-start(bf16[2048,128]{1,0:T(8,128)(2,1)} %collective-permute-done.12), channel_id=1, source_target_pairs={{1,0},{2,1},{3,2},{4,3},{5,4},{6,5},{7,6},{8,7},{9,8},{10,9},{11,1... | collective-permute-start | bytes 1572872 | tf_op jit(solution)/shard_map/ppermute | solution.py:26
  110.5 9.0 %collective-permute-start.7 = (bf16[2048,128]{1,0:T(8,128)(2,1)}, bf16[2048,128]{1,0:T(8,128)(2,1)}, u32[]{:S(2)}, u32[]{:S(2)}) collective-permute-start(bf16[2048,128]{1,0:T(8,128)(2,1)} %collective-permute-done.6), channel_id=1, source_target_pairs={{0,1},{1,2},{2,3},{3,4},{4,5},{5,6},{6,7},{7,8},{8,9},{9,10},{10,1... | collective-permute-start | bytes 1572872 | tf_op jit(solution)/shard_map/ppermute | solution.py:24
  115.8 19.1 %copy-start.4 = (bf16[2048,128]{1,0:T(8,128)(2,1)S(1)}, bf16[2048,128]{1,0:T(8,128)(2,1)}, u32[]{:S(2)}) copy-start(bf16[2048,128]{1,0:T(8,128)(2,1)} %copy-done.3) | copy-start | bytes 1572868
  117.5 23.9 %collective-permute-start.14 = (bf16[2048,128]{1,0:T(8,128)(2,1)}, bf16[2048,128]{1,0:T(8,128)(2,1)S(1)}, u32[]{:S(2)}, u32[]{:S(2)}) collective-permute-start(bf16[2048,128]{1,0:T(8,128)(2,1)} %collective-permute-done.13), channel_id=1, source_target_pairs={{1,0},{2,1},{3,2},{4,3},{5,4},{6,5},{7,6},{8,7},{9,8},{10,9},{11,1... | collective-permute-start | bytes 1572872 | tf_op jit(solution)/shard_map/ppermute | solution.py:26
  163.0 55.3 %copy-start.7 = (f32[16]{0:T(128)S(1)}, f32[16]{0:T(128)}, u32[]{:S(2)}) copy-start(f32[16]{0:T(128)} %param.17) | copy-start | bytes 196
  163.0 55.9 %copy-start.8 = (f32[16]{0:T(128)S(1)}, f32[16]{0:T(128)}, u32[]{:S(2)}) copy-start(f32[16]{0:T(128)} %param.18) | copy-start | bytes 196
  169.6 35.0 %all-to-all-start = ((bf16[128,16,1,128]{0,3,2,1:T(8,128)(2,1)}), bf16[128,16,1,128]{0,3,2,1:T(8,128)(2,1)S(1)}, u32[]{:S(2)}, u32[]{:S(2)}) async-start(bf16[128,16,1,128]{0,3,2,1:T(8,128)(2,1)} %bitcast.22), calls=%async_computation | async-start | bytes 1048576 | tf_op jit(solution)/shard_map/all_to_all | solution.py:91
  205.5 42.4 %all-to-all-start.1 = ((bf16[128,16,1,128]{3,0,2,1:T(8,128)(2,1)}), bf16[128,16,1,128]{3,0,2,1:T(8,128)(2,1)S(1)}, u32[]{:S(2)}, u32[]{:S(2)}) async-start(bf16[128,16,1,128]{3,0,2,1:T(8,128)(2,1)} %bitcast.32), calls=%async_computation.1 | async-start | bytes 1048576 | tf_op jit(solution)/shard_map/all_to_all | solution.py:93
  248.8 35.8 %all-to-all-start.3 = ((bf16[128,16,1,128]{3,0,2,1:T(8,128)(2,1)}), bf16[128,16,1,128]{3,0,2,1:T(8,128)(2,1)S(1)}, u32[]{:S(2)}, u32[]{:S(2)}) async-start(bf16[128,16,1,128]{3,0,2,1:T(8,128)(2,1)} %bitcast.53), calls=%async_computation.3 | async-start | bytes 1048576 | tf_op jit(solution)/shard_map/all_to_all | solution.py:94
Sparse Core Ops, SparseCore 0:
  115.9 48.1 all-gather.1
